TPU v7x, 128 devices: a whole 4x4x4 slice. The times are simulated.
128 devices in a mesh: fs: 16 (over z, y), tp: 8 (over x, core).
Axes of the slice: x: 4, y: 4, z: 4, core: 2. Of those that a mesh axis runs over, the one named last changes fastest.
Arguments:
- tokens: bfloat16 [12288, 2048], P('fs', 'tp'), may hold values from -40 to 40
- gain_one: float32 [2048], P('tp'), may hold values from 0.1 to 1.9
- w_gate: float32 [2048, 3072], P('fs', 'tp'), may hold values from -0.125 to 0.125
- w_up: float32 [2048, 3072], P('fs', 'tp'), may hold values from -0.125 to 0.125
- w_down: float32 [3072, 2048], P('tp', 'fs'), may hold values from -0.109375 to 0.109375
- scale_gate: float32 [3072], P('tp'), may hold values from 0.5 to 2
- scale_up: float32 [3072], P('tp'), may hold values from 0.5 to 2
- scale_down: float32 [2048], P('tp'), may hold values from 0.5 to 2
- gain_mix: float32 [2048], P('tp'), may hold values from 0.1 to 1.9
- w_query: float32 [2048, 2048], P('fs', 'tp'), may hold values from -0.125 to 0.125
- w_key: float32 [2048, 2048], P('fs', 'tp'), may hold values from -0.125 to 0.125
- w_value: float32 [2048, 2048], P('fs', 'tp'), may hold values from -0.125 to 0.125
- w_outgate: float32 [2048, 2048], P('fs', 'tp'), may hold values from -0.125 to 0.125
- scale_query: float32 [2048], P('tp'), may hold values from 0.5 to 2
- scale_key: float32 [2048], P('tp'), may hold values from 0.5 to 2
- scale_value: float32 [2048], P('tp'), may hold values from 0.5 to 2
- scale_outgate: float32 [2048], P('tp'), may hold values from 0.5 to 2
- ret_gain: float32 [2048], P('tp'), may hold values from 0.1 to 1.9
- decay_rate: float32 [8], P('tp'), may hold values from 0 to 2
- w_mix: float32 [2048, 2048], P('tp', 'fs'), may hold values from -0.125 to 0.125
- scale_mix: float32 [2048], P('tp'), may hold values from 0.5 to 2
- gain_two: float32 [2048], P('tp'), may hold values from 0.1 to 1.9
Outputs:
- layer_out: bfloat16 [12288, 2048], P('fs', 'tp')
All inputs are finite; a program needn't handle non-finite values.
Results may differ from a plain program's by a relative error of at most 0.022.
Values may be sent and summed in bfloat16 or wider, within the bound.
A program may use at most 128 MiB of HBM per device.

v0:
```python
import jax
import jax.numpy as jnp
from jax import lax
from jax.sharding import PartitionSpec as P

D = 2048
LEN = 256
BLK = 128
EPS = 1e-06
HEAD_EPS = 0.1


def from_everyone(shard, axis):
    copies = jnp.broadcast_to(shard, (lax.axis_size(axis), *shard.shape))
    return lax.all_to_all(copies, axis, split_axis=0, concat_axis=0, tiled=True)


def taken_together(shard, axis):
    return from_everyone(shard, axis).sum(axis=0)


def in_blocks(shard, dim, length):
    shape = shard.shape
    blocks = shard.reshape(*shape[:dim], length, shape[dim] // length, *shape[dim + 1 :])
    return jnp.moveaxis(blocks, dim, 0)


def sent_and_summed(shard, axis, dim):
    length = lax.axis_size(axis)
    blocks = lax.all_to_all(in_blocks(shard, dim, length), axis, 0, 0, tiled=True)
    return jnp.sum(blocks.astype(jnp.float32), axis=0)


def side_by_side(arrays, axis, dim, along):
    widths = [a.shape[along] for a in arrays]
    both = jnp.concatenate(arrays, axis=along)
    out = lax.all_gather(both, axis, axis=dim, tiled=True)
    return tuple(jnp.split(out, [sum(widths[:k]) for k in range(1, len(widths))], axis=along))


def laid_out(blocks, dim):
    blocks = jnp.moveaxis(blocks, 0, dim)
    shape = blocks.shape
    return blocks.reshape(*shape[:dim], shape[dim] * shape[dim + 1], *shape[dim + 2 :])


def gathered_copies(shard, axis, dim):
    return laid_out(from_everyone(shard, axis), dim)


def rotate_pairs(values):
    paired = values.reshape(values.shape[:-1] + (values.shape[-1] // 2, 2))
    return jnp.stack((-paired[..., 1], paired[..., 0]), axis=-1).reshape(values.shape)


def retain(query_rows, key_rows, value_rows, decay_rate, length, block):
    total_rows = query_rows.shape[0]
    heads = decay_rate.shape[0]
    head_size = query_rows.shape[1] // heads
    sequences = total_rows // length
    nblocks = length // block

    def split_heads(values):
        return values.astype(jnp.float32).reshape(sequences, length, heads, head_size)

    freq = 1.0 / 10000.0 ** jnp.linspace(0.0, 1.0, head_size // 2, dtype=jnp.float32)
    freq = jnp.repeat(freq, 2)
    angles = jnp.arange(length, dtype=jnp.float32)[:, None] * freq[None, :]
    sines = jnp.sin(angles)[None, :, None, :]
    cosines = jnp.cos(angles)[None, :, None, :]
    queries = split_heads(query_rows)
    queries = queries * cosines + rotate_pairs(queries) * sines
    keys_all = split_heads(key_rows) * head_size ** (-0.5)
    keys_all = keys_all * cosines + rotate_pairs(keys_all) * sines
    values_all = split_heads(value_rows)
    log_decay = -decay_rate
    offsets = jnp.arange(block, dtype=jnp.float32)
    distance = offsets[:, None] - offsets[None, :]
    inside = jnp.where(
        distance >= 0, jnp.exp(log_decay[:, None, None] * jnp.maximum(distance, 0.0)), 0.0
    )
    query_decay = jnp.exp(log_decay[None, :] * (offsets[:, None] + 1.0))
    key_decay = jnp.exp(log_decay[None, :] * (block - 1.0 - offsets[:, None]))
    block_decay = jnp.exp(log_decay * block)

    def to_blocks(values):
        return jnp.moveaxis(values.reshape(sequences, nblocks, block, heads, head_size), 1, 0)

    def advance(carried, pieces):
        query_blk, key_blk, value_blk = pieces
        scores = jnp.einsum("snhd,smhd->shnm", query_blk, key_blk) * inside
        within = jnp.einsum("shnm,smhe->snhe", scores, value_blk)
        across = jnp.einsum("snhd,shde->snhe", query_blk, carried) * query_decay[None, :, :, None]
        weighted = key_blk * key_decay[None, :, :, None]
        carried = carried * block_decay[None, :, None, None] + jnp.einsum(
            "smhd,smhe->shde", weighted, value_blk
        )
        return (carried, within + across)

    initial = jnp.zeros((sequences, heads, head_size, head_size), jnp.float32)
    _, results = lax.scan(
        advance, initial, (to_blocks(queries), to_blocks(keys_all), to_blocks(values_all))
    )
    results = jnp.moveaxis(results, 0, 1).reshape(sequences, length, heads, head_size)
    results = results * lax.rsqrt(jnp.mean(results * results, axis=-1, keepdims=True) + HEAD_EPS)
    return results.reshape(total_rows, heads * head_size)


def normed_rows(hidden_in, norm_gain):
    widened = hidden_in.astype(jnp.float32)
    totals = taken_together(jnp.sum(widened * widened, axis=1), "tp")
    scaled = widened * lax.rsqrt(totals / D + EPS)[:, None] * norm_gain
    return lax.all_gather(scaled.astype(jnp.bfloat16), "tp", axis=1, tiled=True)


def summed_share(partial_value):
    rounded = lax.optimization_barrier(partial_value.astype(jnp.bfloat16))
    return sent_and_summed(rounded.astype(jnp.float32).astype(jnp.bfloat16), "tp", 1)


def ffn_gathered(features, gate_low, up_low, down_low, scale_gate, scale_up):
    pieces = side_by_side((gate_low, up_low), "fs", 0, 1)
    gate_add = jnp.dot(features, pieces[0], preferred_element_type=jnp.float32)
    up_add = jnp.dot(features, pieces[1], preferred_element_type=jnp.float32)
    hidden = (jax.nn.silu(gate_add * scale_gate) * (up_add * scale_up)).astype(jnp.bfloat16)
    return jnp.dot(hidden, gathered_copies(down_low, "fs", 1), preferred_element_type=jnp.float32)


def per_device(
    tokens,
    gain_one,
    w_gate,
    w_up,
    w_down,
    scale_gate,
    scale_up,
    scale_down,
    gain_mix,
    w_query,
    w_key,
    w_value,
    w_outgate,
    scale_query,
    scale_key,
    scale_value,
    scale_outgate,
    ret_gain,
    decay_rate,
    w_mix,
    scale_mix,
    gain_two,
):
    norm_one, norm_mix, norm_two, down_cols, mix_cols = (
        gain_one,
        gain_mix,
        gain_two,
        scale_down,
        scale_mix,
    )
    gate_low = w_gate.astype(jnp.bfloat16)
    up_low = w_up.astype(jnp.bfloat16)
    down_low = w_down.astype(jnp.bfloat16)
    ffn_one = ffn_gathered(
        normed_rows(tokens, norm_one), gate_low, up_low, down_low, scale_gate, scale_up
    )
    first = (tokens.astype(jnp.float32) + 0.5 * summed_share(ffn_one) * down_cols).astype(
        jnp.bfloat16
    )
    features = normed_rows(first, norm_mix)
    pieces = side_by_side(
        (
            w_query.astype(jnp.bfloat16),
            w_key.astype(jnp.bfloat16),
            w_value.astype(jnp.bfloat16),
            w_outgate.astype(jnp.bfloat16),
        ),
        "fs",
        0,
        1,
    )
    query_pre, key_pre, value_pre, outgate_pre = tuple(
        (jnp.dot(features, piece, preferred_element_type=jnp.float32) for piece in pieces)
    )
    query_rows = (query_pre * scale_query).astype(jnp.bfloat16)
    key_rows = (key_pre * scale_key).astype(jnp.bfloat16)
    value_rows = (value_pre * scale_value).astype(jnp.bfloat16)
    outgate_rows = (outgate_pre * scale_outgate).astype(jnp.bfloat16)
    retained = retain(query_rows, key_rows, value_rows, decay_rate, LEN, BLK)
    mixed = (retained * ret_gain * jax.nn.silu(outgate_rows.astype(jnp.float32))).astype(
        jnp.bfloat16
    )
    mix_partial = jnp.dot(
        mixed,
        gathered_copies(w_mix.astype(jnp.bfloat16), "fs", 1),
        preferred_element_type=jnp.float32,
    )
    second = (first.astype(jnp.float32) + summed_share(mix_partial) * mix_cols).astype(jnp.bfloat16)
    ffn_two = ffn_gathered(
        normed_rows(second, norm_two), gate_low, up_low, down_low, scale_gate, scale_up
    )
    result = (second.astype(jnp.float32) + 0.5 * summed_share(ffn_two) * down_cols).astype(
        jnp.bfloat16
    )
    return result


def solution(mesh):
    return jax.shard_map(
        per_device,
        mesh=mesh,
        in_specs=(
            P("fs", "tp"),
            P("tp"),
            P("fs", "tp"),
            P("fs", "tp"),
            P("tp", "fs"),
            P("tp"),
            P("tp"),
            P("tp"),
            P("tp"),
            P("fs", "tp"),
            P("fs", "tp"),
            P("fs", "tp"),
            P("fs", "tp"),
            P("tp"),
            P("tp"),
            P("tp"),
            P("tp"),
            P("tp"),
            P("tp"),
            P("tp", "fs"),
            P("tp"),
            P("tp"),
        ),
        out_specs=P("fs", "tp"),
        check_vma=False,
    )
```

profile of v0, /device:TPU:1, one launch (start us, length us, event | category | flops | bytes accessed | tf_op | source)
XLA Modules:
  0.0 379.9 jit_solution(7782225091500418627)
XLA Ops:
  6.6 1.2 fusion.52
  7.9 10.3 %all_to_all.44 = f32[8,1,768]{2,1,0:T(1,128)S(1)} all-to-all(f32[8,1,768]{2,1,0:T(1,128)S(1)} %broadcast_in_dim.23), channel_id=1, replica_groups=mesh['fs'=16,'tp'=8] {'tp'}, dimensions={0} | all-to-all | bytes 49152 | tf_op jit(solution)/shard_map/all_to_all | solution.py:15
  18.2 1.9 fusion.54
  20.2 0.9 convert_element_type.111
  21.1 0.9 convert_element_type.112
  22.1 0.7 pad_maximum_fusion.3
  22.8 0.9 convert_element_type.120
  23.8 0.7 pad_maximum_fusion.2
  24.8 1.3 broadcast_in_dim.24
  26.1 7.8 %all-to-all-start.1 = ((bf16[16,384,128]{1,2,0:T(8,128)(2,1)}), bf16[16,384,128]{1,2,0:T(8,128)(2,1)S(1)}, u32[]{:S(2)}, u32[]{:S(2)}) async-start(bf16[16,384,128]{1,2,0:T(8,128)(2,1)} %broadcast_in_dim.24), calls=%async_computation.1 | async-start | bytes 3145728 | tf_op jit(solution)/shard_map/all_to_all | solution.py:15
  33.9 18.4 %all-gather.6.cloned.1.call-done = bf16[768,2048]{1,0:T(8,128)(2,1)} async-done(((bf16[768,256]{1,0:T(8,128)(2,1)}), bf16[768,2048]{1,0:T(8,128)(2,1)}) %all-gather.6.cloned.1.call-update) | async-done | bytes 3145744 | tf_op jit(solution)/shard_map/all_gather | solution.py:113
  52.3 50.1 %all-gather.8.cloned.1.call-done = bf16[2048,768]{1,0:T(8,128)(2,1)} async-done(((bf16[128,768]{1,0:T(8,128)(2,1)}), bf16[2048,768]{1,0:T(8,128)(2,1)}) %all-gather.8.cloned.1.call-update) | async-done | bytes 3145744 | tf_op jit(solution)/shard_map/all_gather | solution.py:37
  102.4 5.2 %convolution_multiply_fusion.4 = f32[768,384]{1,0:T(8,128)} fusion(bf16[768,2048]{1,0:T(8,128)(2,1)} %all-gather.6.cloned.1.call-done, bf16[2048,768]{1,0:T(8,128)(2,1)} %all-gather.8.cloned.1.call-done, f32[384]{0:T(512)S(1)} %copy-done.21), kind=kOutput, calls=%fused_computation.47 | convolution fusion | flops 1208254464 | bytes 5899776 | tf_op jit(solution)/shard_map/dot_general | solution.py:123
  107.6 1.1 copy-done.7
  108.8 6.7 %convolution_convert_fusion.2 = bf16[768,2048]{1,0:T(8,128)(2,1)S(1)} fusion(bf16[384,2048]{0,1:T(8,128)(2,1)} %bitcast.163, bf16[768,2048]{1,0:T(8,128)(2,1)} %all-gather.6.cloned.1.call-done, bf16[2048,768]{1,0:T(8,128)(2,1)} %all-gather.8.cloned.1.call-done, f32[768,384]{1,0:T(8,128)} %convolution_multiply_fusion.4, f32[384]{0:T(512)S(1)} %copy-done.22), kind=kOutput, calls=%fused_computation.38 | convolution fusion | flops 2419556352 | bytes 10618368 | tf_op jit(solution)/shard_map/dot_general | solution.py:126
  115.4 2.0 copy.141
  117.4 5.7 %all-to-all-start.2 = ((bf16[8,768,256]{2,1,0:T(8,128)(2,1)}), bf16[8,768,256]{2,1,0:T(8,128)(2,1)S(1)}, u32[]{:S(2)}, u32[]{:S(2)}) async-start(bf16[8,768,256]{2,1,0:T(8,128)(2,1)} %bitcast.116), calls=%async_computation.2 | async-start | bytes 6291456 | tf_op jit(solution)/shard_map/all_to_all | solution.py:30
  123.1 37.4 %all-to-all-done.2 = bf16[8,768,256]{2,1,0:T(8,128)(2,1)S(1)} async-done(((bf16[8,768,256]{2,1,0:T(8,128)(2,1)}), bf16[8,768,256]{2,1,0:T(8,128)(2,1)S(1)}, u32[]{:S(2)}, u32[]{:S(2)}) %all-to-all-start.2) | async-done | bytes 3145760 | tf_op jit(solution)/shard_map/all_to_all | solution.py:30
  160.5 0.4 convert_reduce_fusion.2
  161.2 8.0 %all_to_all.45 = f32[8,1,768]{2,1,0:T(1,128)S(1)} all-to-all(f32[8,1,768]{2,1,0:T(1,128)S(1)} %broadcast_in_dim.27), channel_id=1, replica_groups=mesh['fs'=16,'tp'=8] {'tp'}, dimensions={0} | all-to-all | bytes 49152 | tf_op jit(solution)/shard_map/all_to_all | solution.py:15
  169.3 0.9 fusion.58
  170.2 0.9 convert_element_type.132
  171.3 1.1 broadcast_in_dim.31
  172.3 4.3 %all-to-all-start.4 = ((bf16[16,256,128]{1,2,0:T(8,128)(2,1)}), bf16[16,256,128]{1,2,0:T(8,128)(2,1)}, u32[]{:S(2)}, u32[]{:S(2)}) async-start(bf16[16,256,128]{1,2,0:T(8,128)(2,1)} %broadcast_in_dim.31), calls=%async_computation.4 | async-start | bytes 2097152 | tf_op jit(solution)/shard_map/all_to_all | solution.py:15
  178.0 8.5 %multiply_cosine_fusion = (f32[2,128,256]{1,0,2:T(2,128)}, f32[2,128,256]{1,0,2:T(2,128)}, f32[2,128,256]{1,0,2:T(2,128)}) fusion(f32[2,128]{1,0:T(2,128)S(1)} %multiply_add_fusion, f32[256]{0:T(256)S(1)} %mul.470), kind=kLoop, calls=%fused_computation.107 | loop fusion | flops 327680 | bytes 788480 | tf_op jit(solution)/shard_map/cos | solution.py:70
  186.5 12.2 %all-gather.10.cloned.1.call-done = bf16[768,2048]{1,0:T(8,128)(2,1)} async-done(((bf16[768,256]{1,0:T(8,128)(2,1)}), bf16[768,2048]{1,0:T(8,128)(2,1)}) %all-gather.10.cloned.1.call-update) | async-done | bytes 3145744 | tf_op jit(solution)/shard_map/all_gather | solution.py:113
  198.7 4.1 %broadcast_multiply_fusion = (f32[768,256]{1,0:T(8,128)S(1)}, f32[768,256]{1,0:T(8,128)}) fusion(f32[256]{0:T(256)S(1)} %copy-done.24, bf16[768,2048]{1,0:T(8,128)(2,1)} %all-gather.10.cloned.1.call-done, bf16[2048,1024]{1,0:T(8,128)(2,1)} %all-gather.12.cloned.1.call-done), kind=kOutput, calls=%fused_computation.106 | convolution fusion | flops 806092800 | bytes 5768192 | tf_op jit(solution)/shard_map/dot_general | solution.py:182
  202.8 0.3 copy.108
  203.1 0.4 mul.479
  204.0 1.7 copy.109
  205.7 2.2 fusion.41
  207.9 0.3 copy.112
  208.2 0.4 reshape_reshape.8
  209.1 1.7 copy.113
  210.8 1.2 copy.107
  212.0 1.2 copy.111
  213.3 3.3 fusion.39
  216.7 1.9 add_bitcast_fusion
  218.5 8.8 %while.15 = (s32[]{:T(128)}, f32[3,1,256,256]{3,2,0,1:T(8,128)S(1)}, f32[2,3,128,1,256]{2,4,1,3,0:T(8,128)}, f32[1]{0:T(128)}, f32[2,3,128,1,256]{2,0,3,4,1:T(2,...) while((s32[]{:T(128)}, ...), condition=%wide.region_6.7_spmd.clone.clone.clone, body=%wide.region_5.6_spmd.clone.clone.clone.sunk | while | flops 152257024 | bytes 7998088 | solution.py:101
  218.5 2.0 constant_dynamic-slice_fusion.3
  220.6 0.4 convolution_bitcast_fusion.4
  221.0 1.1 fusion.108
  222.1 0.3 copy.144
  222.4 0.4 fusion.107
  222.8 1.9 constant_dynamic-slice_fusion.3
  224.8 0.4 convolution_bitcast_fusion.4
  225.3 1.1 fusion.108
  226.4 0.3 copy.144
  226.7 0.4 fusion.107
  227.3 1.4 copy.116
  228.8 1.2 multiply_reduce_fusion
  230.0 3.2 fusion.66
  233.3 2.2 convolution_convert_fusion.1
  235.7 41.4 %all_to_all.46 = bf16[8,768,256]{2,1,0:T(8,128)(2,1)S(1)} all-to-all(bf16[8,768,256]{2,1,0:T(8,128)(2,1)S(1)} %bitcast.155), channel_id=1, replica_groups=mesh['fs'=16,'tp'=8] {'tp'}, dimensions={0} | all-to-all | bytes 6291456 | tf_op jit(solution)/shard_map/all_to_all | solution.py:30
  277.1 0.4 convert_reduce_fusion.1
  277.6 0.5 copy-done.2
  278.4 8.1 %all_to_all.47 = f32[8,1,768]{2,1,0:T(1,128)S(1)} all-to-all(f32[8,1,768]{2,1,0:T(1,128)S(1)} %broadcast_in_dim.32), channel_id=1, replica_groups=mesh['fs'=16,'tp'=8] {'tp'}, dimensions={0} | all-to-all | bytes 49152 | tf_op jit(solution)/shard_map/all_to_all | solution.py:15
  286.5 0.9 fusion.62
  287.5 31.1 %all-gather.14.cloned.1.call-done = bf16[768,2048]{1,0:T(8,128)(2,1)} async-done(((bf16[768,256]{1,0:T(8,128)(2,1)}), bf16[768,2048]{1,0:T(8,128)(2,1)}) %all-gather.14.cloned.1.call-update) | async-done | bytes 3145744 | tf_op jit(solution)/shard_map/all_gather | solution.py:113
  318.6 5.3 %convolution_multiply_fusion.2 = f32[768,384]{1,0:T(8,128)} fusion(bf16[768,2048]{1,0:T(8,128)(2,1)} %all-gather.14.cloned.1.call-done, bf16[2048,768]{1,0:T(8,128)(2,1)} %all-gather.8.cloned.1.call-done, f32[384]{0:T(512)S(1)} %copy-done.21), kind=kOutput, calls=%fused_computation.44 | convolution fusion | flops 1208254464 | bytes 5899776 | tf_op jit(solution)/shard_map/dot_general | solution.py:123
  323.8 6.6 %convolution_convert_fusion = bf16[768,2048]{1,0:T(8,128)(2,1)S(1)} fusion(bf16[384,2048]{0,1:T(8,128)(2,1)} %bitcast.164, bf16[768,2048]{1,0:T(8,128)(2,1)} %all-gather.14.cloned.1.call-done, bf16[2048,768]{1,0:T(8,128)(2,1)} %all-gather.8.cloned.1.call-done, f32[768,384]{1,0:T(8,128)} %convolution_multiply_fusion.2, f32[384]{0:T(512)S(1)} %copy-done.23), kind=kOutput, calls=%fused_computation.36 | convolution fusion | flops 2419556352 | bytes 10618368 | tf_op jit(solution)/shard_map/dot_general | solution.py:126
  330.7 41.4 %all_to_all.48 = bf16[8,768,256]{2,1,0:T(8,128)(2,1)S(1)} all-to-all(bf16[8,768,256]{2,1,0:T(8,128)(2,1)S(1)} %bitcast.156), channel_id=1, replica_groups=mesh['fs'=16,'tp'=8] {'tp'}, dimensions={0} | all-to-all | bytes 6291456 | tf_op jit(solution)/shard_map/all_to_all | solution.py:30
  372.1 0.4 convert_reduce_fusion
  372.5 0.9 fusion.63
  (108 shorter events, 3.2 us)
Async XLA Ops:
  6.5 17.2 %copy-start.13 = (f32[128,256]{1,0:T(8,128)S(1)}, f32[128,256]{1,0:T(8,128)}, u32[]{:S(2)}) copy-start(f32[128,256]{1,0:T(8,128)} %param.34) | copy-start | bytes 393220
  6.5 17.2 %copy-start.14 = (f32[128,256]{1,0:T(8,128)S(1)}, f32[128,256]{1,0:T(8,128)}, u32[]{:S(2)}) copy-start(f32[128,256]{1,0:T(8,128)} %param.35) | copy-start | bytes 393220
  6.5 17.3 %copy-start.15 = (f32[128,256]{1,0:T(8,128)S(1)}, f32[128,256]{1,0:T(8,128)}, u32[]{:S(2)}) copy-start(f32[128,256]{1,0:T(8,128)} %param.36) | copy-start | bytes 393220
  6.5 18.1 %copy-start.12 = (f32[384,128]{1,0:T(8,128)S(1)}, f32[384,128]{1,0:T(8,128)}, u32[]{:S(2)}) copy-start(f32[384,128]{1,0:T(8,128)} %param.28) | copy-start | bytes 589828
  6.5 45.8 %all-gather.6.cloned.1.call-start = ((), (), s32[]{:S(2)}) async-start(), calls=%async_computation.8 | async-start | bytes 3538944 | tf_op jit(solution)/shard_map/all_gather | solution.py:113
  20.1 82.3 %all-gather.8.cloned.1.call-start = ((), (), s32[]{:S(2)}) async-start(), calls=%async_computation.9 | async-start | bytes 3342336 | tf_op jit(solution)/shard_map/all_gather | solution.py:37
  22.8 163.7 %all-gather.12.cloned.1.call-start = ((), (), s32[]{:S(2)}) async-start(), calls=%async_computation.11 | async-start | bytes 4456448 | tf_op jit(solution)/shard_map/all_gather | solution.py:37
  23.8 78.6 %copy-start.21 = (f32[384]{0:T(512)S(1)}, f32[384]{0:T(512)}, u32[]{:S(2)}) copy-start(f32[384]{0:T(512)} %param.29) | copy-start | bytes 4612
  26.1 81.5 %all-to-all-start.1 = ((bf16[16,384,128]{1,2,0:T(8,128)(2,1)}), bf16[16,384,128]{1,2,0:T(8,128)(2,1)S(1)}, u32[]{:S(2)}, u32[]{:S(2)}) async-start(bf16[16,384,128]{1,2,0:T(8,128)(2,1)} %broadcast_in_dim.24), calls=%async_computation.1 | async-start | bytes 3145728 | tf_op jit(solution)/shard_map/all_to_all | solution.py:15
  33.9 74.9 %copy-start.22 = (f32[384]{0:T(512)S(1)}, f32[384]{0:T(512)}, u32[]{:S(2)}) copy-start(f32[384]{0:T(512)} %param.30) | copy-start | bytes 4612
  107.6 1.1 copy-start.7
  117.4 5.7 %copy-start.18 = (f32[256]{0:T(256)S(1)}, f32[256]{0:T(256)}, u32[]{:S(2)}) copy-start(f32[256]{0:T(256)} %param.31) | copy-start | bytes 3076
  117.4 43.1 %all-to-all-start.2 = ((bf16[8,768,256]{2,1,0:T(8,128)(2,1)}), bf16[8,768,256]{2,1,0:T(8,128)(2,1)S(1)}, u32[]{:S(2)}, u32[]{:S(2)}) async-start(bf16[8,768,256]{2,1,0:T(8,128)(2,1)} %bitcast.116), calls=%async_computation.2 | async-start | bytes 6291456 | tf_op jit(solution)/shard_map/all_to_all | solution.py:30
  123.1 37.9 %copy-start = (bf16[768,256]{1,0:T(8,128)(2,1)S(1)}, bf16[768,256]{1,0:T(8,128)(2,1)}, u32[]{:S(2)}) copy-start(bf16[768,256]{1,0:T(8,128)(2,1)} %param.24) | copy-start | bytes 1179652
  123.1 46.2 %copy-start.16 = (f32[256]{0:T(256)S(1)}, f32[256]{0:T(256)}, u32[]{:S(2)}) copy-start(f32[256]{0:T(256)} %param.32) | copy-start | bytes 3076
  123.1 75.6 %all-gather.10.cloned.1.call-start = ((), (), s32[]{:S(2)}) async-start(), calls=%async_computation.10 | async-start | bytes 3538944 | tf_op jit(solution)/shard_map/all_gather | solution.py:113
  161.2 15.5 %copy-start.1 = (bf16[768,256]{1,0:T(8,128)(2,1)}, bf16[768,256]{1,0:T(8,128)(2,1)S(1)}, u32[]{:S(2)}) copy-start(bf16[768,256]{1,0:T(8,128)(2,1)S(1)} %get-tuple-element.210) | copy-start | bytes 1179652
  161.2 37.5 %copy-start.24 = (f32[256]{0:T(256)S(1)}, f32[256]{0:T(256)}, u32[]{:S(2)}) copy-start(f32[256]{0:T(256)} %param.38) | copy-start | bytes 3076
  172.3 60.9 %all-to-all-start.4 = ((bf16[16,256,128]{1,2,0:T(8,128)(2,1)}), bf16[16,256,128]{1,2,0:T(8,128)(2,1)}, u32[]{:S(2)}, u32[]{:S(2)}) async-start(bf16[16,256,128]{1,2,0:T(8,128)(2,1)} %broadcast_in_dim.31), calls=%async_computation.4 | async-start | bytes 2097152 | tf_op jit(solution)/shard_map/all_to_all | solution.py:15
  176.7 141.9 %all-gather.14.cloned.1.call-start = ((), (), s32[]{:S(2)}) async-start(), calls=%async_computation.12 | async-start | bytes 3538944 | tf_op jit(solution)/shard_map/all_gather | solution.py:113
  203.5 2.2 copy-start.20
  203.5 2.2 copy-start.25
  208.6 2.2 copy-start.11
  208.9 4.3 %copy-start.26 = (f32[256]{0:T(256)S(1)}, f32[256]{0:T(256)}, u32[]{:S(2)}) copy-start(f32[256]{0:T(256)} %param.39) | copy-start | bytes 3076
  213.2 3.4 copy-start.3
  213.2 3.4 copy-start.4
  213.2 3.4 copy-start.5
  213.2 3.4 copy-start.6
  213.2 3.4 copy-start.8
  213.2 3.4 copy-start.9
  213.2 3.4 copy-start.10
  218.5 11.5 %copy-start.27 = (f32[256]{0:T(256)S(1)}, f32[256]{0:T(256)}, u32[]{:S(2)}) copy-start(f32[256]{0:T(256)} %param.40) | copy-start | bytes 3076
  218.5 11.5 %copy-start.28 = (f32[256]{0:T(256)S(1)}, f32[256]{0:T(256)}, u32[]{:S(2)}) copy-start(f32[256]{0:T(256)} %param.41) | copy-start | bytes 3076
  277.1 1.0 copy-start.2
  277.1 1.0 copy-start.19
  277.1 9.4 %copy-start.17 = (f32[256]{0:T(256)S(1)}, f32[256]{0:T(256)}, u32[]{:S(2)}) copy-start(f32[256]{0:T(256)} %param.45) | copy-start | bytes 3076
  287.4 36.4 %copy-start.23 = (f32[384]{0:T(512)S(1)}, f32[384]{0:T(512)}, u32[]{:S(2)}) copy-start(f32[384]{0:T(512)} %param.30) | copy-start | bytes 4612
Sparse Core Ops, SparseCore 0:
  20.2 32.0 all-gather.5
  54.5 47.8 all-gather.7
  104.5 50.5 all-gather.11
  170.3 28.3 all-gather.9
  287.6 30.9 all-gather.13
where the time goes:
time: 381 us; the launch traced here: 380 us
  waiting for transfers between devices  149 us (39%)
  blocking collectives  109 us (29%)
  matrix products  42.7 us (11%)
  other arithmetic  25.7 us (7%)
  local copies, waits for them, and re-layouts  20.2 us (5%)
  starting transfers between devices  18.2 us (5%)
  between operations  14.5 us (4%)
    all_to_all x2, blocking collectives, sent_and_summed(): lax.all_to_all(in_blocks(shard, dim, length), axis, 0, 0, tiled=True)  82.8 us
    all_gather x3, waiting for transfers between devices, normed_rows(): return lax.all_gather(scaled.astype(jnp.bfloat16), 'tp', axis=1, tiled=True)  61.7 us
    all_gather x2, waiting for transfers between devices, side_by_side(): out = lax.all_gather(both, axis, axis=dim, tiled=True)  50.1 us
    all_to_all x1, waiting for transfers between devices, sent_and_summed(): lax.all_to_all(in_blocks(shard, dim, length), axis, 0, 0, tiled=True)  37.4 us
    all_to_all x3, blocking collectives, from_everyone(): return lax.all_to_all(copies, axis, split_axis=0, concat_axis=0, tiled=True)  26.4 us
    dot_general x2, matrix products, ffn_gathered(): jnp.dot(hidden, gathered_copies(down_low, 'fs', 1), preferred_element_typ...  13.3 us
    dot_general x4, matrix products, per_device(): jnp.dot(features, piece, preferred_element_type=jnp.float32)  12.8 us
    all_to_all x2, starting transfers between devices, from_everyone(): return lax.all_to_all(copies, axis, split_axis=0, concat_axis=0, tiled=True)  12.1 us
  transfers between devices with their start and end apart: 8, of which 5 were waited for; matrix products, arithmetic and copies ran while one was open for 17% of the time, Pallas kernels for 0%

commit v1 on v0

--- a/solution.py
+++ b/solution.py
@@ -8,6 +8,12 @@
 BLK = 128
 EPS = 1e-06
 HEAD_EPS = 0.1
+
+
+def _read_cube(field, where_dim):
+    low = list(field.shape[1:])
+    low[where_dim] *= field.shape[0]
+    return jnp.moveaxis(field, 0, where_dim).reshape(low)
 
 
 def from_everyone(shard, axis):
@@ -107,10 +113,32 @@
 
 
 def normed_rows(hidden_in, norm_gain):
+
+    def check_bench(xx, which_axis, dim_k):
+        axis_total = lax.psum(1, which_axis)
+        grid = list(map(lambda s: (s, (s + 1) % axis_total), range(axis_total)))
+        by_rank = [(tick, p) for p, tick in grid]
+        then, state_now = ([], [])
+        u = 0
+        while u < axis_total - 1:
+            if u % 2 == 0:
+                spare = lax.ppermute(then[-1] if then else xx, which_axis, grid)
+                then.append(spare)
+            else:
+                state_now.append(
+                    lax.ppermute(state_now[-1] if state_now else xx, which_axis, by_rank)
+                )
+            u += 1
+        back = jnp.stack([*then[::-1], xx, *state_now], axis=0)
+        z = lax.axis_index(which_axis)
+        field_out = z - len(then)
+        back = back[(jnp.arange(axis_total) - field_out) % axis_total]
+        return _read_cube(back, dim_k)
+
     widened = hidden_in.astype(jnp.float32)
     totals = taken_together(jnp.sum(widened * widened, axis=1), "tp")
     scaled = widened * lax.rsqrt(totals / D + EPS)[:, None] * norm_gain
-    return lax.all_gather(scaled.astype(jnp.bfloat16), "tp", axis=1, tiled=True)
+    return check_bench(scaled.astype(jnp.bfloat16), "tp", 1)
 
 
 def summed_share(partial_value):

time: 381 us -> 403 us (1.058)
  waiting for transfers between devices: 149 us -> 70 us
  starting transfers between devices: 18.2 us -> 64.8 us
  local copies, waits for them, and re-layouts: 20.2 us -> 62.4 us
  blocking collectives: 109 us -> 118 us
    all_gather x3 -> x0, waiting for transfers between devices: 61.7 us -> none  [normed_rows(): return lax.all_gather(scaled.astype(jnp.bfloat16), 'tp', axis=1, tiled=True)]
    all_gather x2, waiting for transfers between devices: 50.1 us -> 0.01 us  [side_by_side(): out = lax.all_gather(both, axis, axis=dim, tiled=True)]
    ppermute x0 -> x21, starting transfers between devices: none -> 41.5 us  [the longest x12 22.6 us: check_bench(): spare = lax.ppermute(then[-1] if then else xx, which_axis, grid)]
    ppermute x0 -> x21, waiting for transfers between devices: none -> 32.6 us  [the longest x12 31.4 us: check_bench(): spare = lax.ppermute(then[-1] if then else xx, which_axis, grid)]
    unnamed x58 -> x82, local copies, waits for them, and re-layouts: 1.8 us -> 15 us
    transpose x0 -> x3, local copies, waits for them, and re-layouts: none -> 10.5 us  [_read_cube(): return jnp.moveaxis(field, 0, where_dim).reshape(low)]
    gather x0 -> x3, local copies, waits for them, and re-layouts: none -> 9.65 us  [check_bench(): back = back[(jnp.arange(axis_total) - field_out) % axis_total]]
    all_to_all x2, blocking collectives: 82.8 us -> 91.1 us  [sent_and_summed(): lax.all_to_all(in_blocks(shard, dim, length), axis, 0, 0, tiled=True)]
  transfers between devices with their start and end apart: 8 -> 26, of which waited for: 5 -> 13; matrix products, arithmetic and copies ran while one was open for 17% -> 26% of each run, Pallas kernels for 0% -> 0%
where the time goes in v1:
time: 403 us; the launch traced here: 402 us
  blocking collectives  118 us (29%)
  waiting for transfers between devices  70 us (17%)
  starting transfers between devices  64.8 us (16%)
  local copies, waits for them, and re-layouts  62.4 us (15%)
  matrix products  44.7 us (11%)
  other arithmetic  27.4 us (7%)
  between operations  14.8 us (4%)
    all_to_all x2, blocking collectives, sent_and_summed(): lax.all_to_all(in_blocks(shard, dim, length), axis, 0, 0, tiled=True)  91.1 us
    all_to_all x1, waiting for transfers between devices, sent_and_summed(): lax.all_to_all(in_blocks(shard, dim, length), axis, 0, 0, tiled=True)  37.4 us
    ppermute x12, waiting for transfers between devices, check_bench(): spare = lax.ppermute(then[-1] if then else xx, which_axis, grid)  31.4 us
    all_to_all x3, blocking collectives, from_everyone(): return lax.all_to_all(copies, axis, split_axis=0, concat_axis=0, tiled=True)  26.5 us
    ppermute x12, starting transfers between devices, check_bench(): spare = lax.ppermute(then[-1] if then else xx, which_axis, grid)  22.6 us
    ppermute x9, starting transfers between devices, check_bench(): lax.ppermute(state_now[-1] if state_now else xx, which_axis, by_rank)  18.9 us
    unnamed x82, local copies, waits for them, and re-layouts  15 us
    dot_general x2, matrix products, ffn_gathered(): jnp.dot(hidden, gathered_copies(down_low, 'fs', 1), preferred_element_typ...  14.8 us
  transfers between devices with their start and end apart: 26, of which 13 were waited for; matrix products, arithmetic and copies ran while one was open for 26% of the time, Pallas kernels for 0%

profile of v1, /device:TPU:1, one launch (start us, length us, event | category | flops | bytes accessed | tf_op | source)
XLA Modules:
  0.0 401.8 jit_solution(2769023523494886376)
XLA Ops:
  9.1 1.2 fusion.52
  10.4 10.4 %all_to_all.44 = f32[8,1,768]{2,1,0:T(1,128)S(1)} all-to-all(f32[8,1,768]{2,1,0:T(1,128)S(1)} %broadcast_in_dim.23), channel_id=1, replica_groups=mesh['fs'=16,'tp'=8] {'tp'}, dimensions={0} | all-to-all | bytes 49152 | tf_op jit(solution)/shard_map/all_to_all | solution.py:21
  20.8 1.2 fusion.54
  23.0 4.7 %collective-permute-done = bf16[768,256]{1,0:T(8,128)(2,1)S(1)} collective-permute-done((bf16[768,256]{1,0:T(8,128)(2,1)S(1)}, bf16[768,256]{1,0:T(8,128)(2,1)S(1)}, u32[]{:S(2)}, u32[]{:S(2)}) %collective-permute-start) | collective-permute-done | bytes 393248 | tf_op jit(solution)/shard_map/ppermute | solution.py:125
  27.7 2.5 collective-permute-start.1
  31.2 3.7 collective-permute-done.1
  34.9 2.5 collective-permute-start.2
  37.7 2.0 collective-permute-start.5
  39.6 2.5 collective-permute-done.2
  42.1 2.5 collective-permute-start.3
  45.6 1.4 broadcast_in_dim.24
  47.0 7.8 %all-to-all-start.1 = ((bf16[16,384,128]{1,2,0:T(8,128)(2,1)}), bf16[16,384,128]{1,2,0:T(8,128)(2,1)}, u32[]{:S(2)}, u32[]{:S(2)}) async-start(bf16[16,384,128]{1,2,0:T(8,128)(2,1)} %broadcast_in_dim.24), calls=%async_computation.1 | async-start | bytes 3145728 | tf_op jit(solution)/shard_map/all_to_all | solution.py:21
  55.9 3.8 collective-permute-start.6
  66.1 2.6 gather_fusion
  68.8 2.9 copy.131
  71.7 5.4 %convolution_multiply_fusion.4 = f32[768,384]{1,0:T(8,128)} fusion(bf16[768,2048]{0,1:T(8,128)(2,1)} %bitcast.220, bf16[2048,768]{1,0:T(8,128)(2,1)} %all-gather.3.cloned.1.call-done, f32[384]{0:T(512)S(1)} %copy-done.23), kind=kOutput, calls=%fused_computation.50 | convolution fusion | flops 1208254464 | bytes 5899776 | tf_op jit(solution)/shard_map/dot_general | solution.py:151
  77.1 7.5 %convolution_convert_fusion.2 = bf16[768,2048]{1,0:T(8,128)(2,1)} fusion(bf16[384,2048]{0,1:T(8,128)(2,1)} %bitcast.12, bf16[768,2048]{0,1:T(8,128)(2,1)S(1)} %bitcast.221, bf16[2048,768]{1,0:T(8,128)(2,1)} %all-gather.3.cloned.1.call-done, f32[768,384]{1,0:T(8,128)} %convolution_multiply_fusion.4, f32[384]{0:T(512)S(1)} %copy-done.25), kind=kOutput, calls=%fused_computation.41 | convolution fusion | flops 2419556352 | bytes 10618368 | tf_op jit(solution)/shard_map/dot_general | solution.py:154
  84.6 3.9 copy.171
  88.5 10.9 %all-to-all-start.2 = ((bf16[8,768,256]{2,1,0:T(8,128)(2,1)}), bf16[8,768,256]{2,1,0:T(8,128)(2,1)S(1)}, u32[]{:S(2)}, u32[]{:S(2)}) async-start(bf16[8,768,256]{2,1,0:T(8,128)(2,1)} %bitcast.172), calls=%async_computation.2 | async-start | bytes 6291456 | tf_op jit(solution)/shard_map/all_to_all | solution.py:36
  99.4 37.4 %all-to-all-done.2 = bf16[8,768,256]{2,1,0:T(8,128)(2,1)S(1)} async-done(((bf16[8,768,256]{2,1,0:T(8,128)(2,1)}), bf16[8,768,256]{2,1,0:T(8,128)(2,1)S(1)}, u32[]{:S(2)}, u32[]{:S(2)}) %all-to-all-start.2) | async-done | bytes 3145760 | tf_op jit(solution)/shard_map/all_to_all | solution.py:36
  137.5 8.0 %all_to_all.45 = f32[8,1,768]{2,1,0:T(1,128)S(1)} all-to-all(f32[8,1,768]{2,1,0:T(1,128)S(1)} %broadcast_in_dim.27), channel_id=1, replica_groups=mesh['fs'=16,'tp'=8] {'tp'}, dimensions={0} | all-to-all | bytes 49152 | tf_op jit(solution)/shard_map/all_to_all | solution.py:21
  146.7 4.7 %collective-permute-done.7 = bf16[768,256]{1,0:T(8,128)(2,1)S(1)} collective-permute-done((bf16[768,256]{1,0:T(8,128)(2,1)S(1)}, bf16[768,256]{1,0:T(8,128)(2,1)S(1)}, u32[]{:S(2)}, u32[]{:S(2)}) %collective-permute-start.7) | collective-permute-done | bytes 393248 | tf_op jit(solution)/shard_map/ppermute | solution.py:125
  151.4 2.5 collective-permute-start.8
  154.9 3.7 collective-permute-done.8
  158.6 2.5 collective-permute-start.9
  163.2 4.5 %all-to-all-start.4 = ((bf16[16,256,128]{1,2,0:T(8,128)(2,1)}), bf16[16,256,128]{1,2,0:T(8,128)(2,1)}, u32[]{:S(2)}, u32[]{:S(2)}) async-start(bf16[16,256,128]{1,2,0:T(8,128)(2,1)} %broadcast_in_dim.29), calls=%async_computation.4 | async-start | bytes 2097152 | tf_op jit(solution)/shard_map/all_to_all | solution.py:21
  167.7 2.3 collective-permute-start.12
  170.7 1.4 broadcast_in_dim.28
  172.0 1.6 mul.470
  174.3 9.2 %multiply_cosine_fusion = (f32[2,128,256]{1,0,2:T(2,128)}, f32[2,128,256]{1,0,2:T(2,128)}, f32[2,128,256]{1,0,2:T(2,128)}) fusion(f32[2,128]{1,0:T(2,128)S(1)} %multiply_add_fusion, f32[256]{0:T(256)} %mul.470), kind=kLoop, calls=%fused_computation.134 | loop fusion | flops 327680 | bytes 788480 | tf_op jit(solution)/shard_map/cos | solution.py:76
  183.5 3.0 collective-permute-start.13
  193.0 4.4 %gather_fusion.1 = bf16[8,768,256]{2,1,0:T(8,128)(2,1)} fusion(bf16[8,768,256]{2,1,0:T(8,128)(2,1)} %bitcast_dynamic-update-slice_fusion.8, s32[1024]{0:T(1024)S(1)} %pad_clamp_fusion), kind=kCustom, calls=%fused_computation.1 | custom fusion | bytes 6291488 | tf_op jit(solution)/shard_map/gather | solution.py:135
  197.4 4.8 %copy.135 = bf16[768,8,256]{0,2,1:T(8,128)(2,1)} copy(bf16[768,8,256]{2,0,1:T(8,128)(2,1)} %bitcast.213) | data formatting | bytes 6291456 | tf_op jit(solution)/shard_map/transpose | solution.py:16
  202.2 4.2 %broadcast_multiply_fusion = (f32[768,256]{1,0:T(8,128)S(1)}, f32[768,256]{1,0:T(8,128)}) fusion(f32[256]{0:T(256)S(1)} %copy-done.27, bf16[768,2048]{0,1:T(8,128)(2,1)} %bitcast.216, bf16[2048,1024]{1,0:T(8,128)(2,1)} %all-gather.5.cloned.1.call-done), kind=kOutput, calls=%fused_computation.133 | convolution fusion | flops 806092800 | bytes 5768192 | tf_op jit(solution)/shard_map/dot_general | solution.py:210
  207.5 1.7 copy.138
  209.3 2.2 fusion.41
  212.7 1.7 copy.142
  215.5 1.2 copy.140
  216.8 3.3 fusion.39
  220.2 1.8 add_bitcast_fusion
  222.0 8.6 %while.15 = (s32[]{:T(128)}, f32[3,1,256,256]{3,2,0,1:T(8,128)S(1)}, f32[2,3,128,1,256]{2,4,1,3,0:T(8,128)}, f32[1]{0:T(128)}, f32[2,3,128,1,256]{2,0,3,4,1:T(2,...) while((s32[]{:T(128)}, ...), condition=%wide.region_6.7_spmd.clone.clone.clone, body=%wide.region_5.6_spmd.clone.clone.clone.sunk | while | flops 152257024 | bytes 7998088 | solution.py:107
  222.0 2.0 constant_dynamic-slice_fusion.3
  226.4 1.9 constant_dynamic-slice_fusion.3
  230.6 1.4 copy.145
  232.0 1.2 multiply_reduce_fusion
  233.3 3.3 fusion.66
  236.6 2.2 convolution_convert_fusion.1
  239.1 44.1 %all_to_all.46 = bf16[8,768,256]{2,1,0:T(8,128)(2,1)S(1)} all-to-all(bf16[8,768,256]{2,1,0:T(8,128)(2,1)S(1)} %bitcast.214), channel_id=1, replica_groups=mesh['fs'=16,'tp'=8] {'tp'}, dimensions={0} | all-to-all | bytes 6291456 | tf_op jit(solution)/shard_map/all_to_all | solution.py:36
  284.4 8.1 %all_to_all.47 = f32[8,1,768]{2,1,0:T(1,128)S(1)} all-to-all(f32[8,1,768]{2,1,0:T(1,128)S(1)} %broadcast_in_dim.32), channel_id=1, replica_groups=mesh['fs'=16,'tp'=8] {'tp'}, dimensions={0} | all-to-all | bytes 49152 | tf_op jit(solution)/shard_map/all_to_all | solution.py:21
  293.6 4.7 %collective-permute-done.14 = bf16[768,256]{1,0:T(8,128)(2,1)S(1)} collective-permute-done((bf16[768,256]{1,0:T(8,128)(2,1)S(1)}, bf16[768,256]{1,0:T(8,128)(2,1)S(1)}, u32[]{:S(2)}, u32[]{:S(2)}) %collective-permute-start.14) | collective-permute-done | bytes 393248 | tf_op jit(solution)/shard_map/ppermute | solution.py:125
  298.3 2.5 collective-permute-start.15
  301.8 3.7 collective-permute-done.15
  305.5 2.5 collective-permute-start.16
  308.3 2.0 collective-permute-start.19
  310.3 2.5 collective-permute-done.16
  312.7 2.5 collective-permute-start.17
  315.8 2.9 collective-permute-start.20
  318.7 1.3 collective-permute-done.17
  326.3 2.6 gather_fusion.2
  329.0 2.8 copy.150
  331.8 5.4 %convolution_multiply_fusion.2 = f32[768,384]{1,0:T(8,128)} fusion(bf16[768,2048]{0,1:T(8,128)(2,1)} %bitcast.222, bf16[2048,768]{1,0:T(8,128)(2,1)} %all-gather.3.cloned.1.call-done, f32[384]{0:T(512)S(1)} %copy-done.24), kind=kOutput, calls=%fused_computation.47 | convolution fusion | flops 1208254464 | bytes 5899776 | tf_op jit(solution)/shard_map/dot_general | solution.py:151
  337.2 7.3 %convolution_convert_fusion = bf16[768,2048]{1,0:T(8,128)(2,1)} fusion(bf16[384,2048]{0,1:T(8,128)(2,1)} %bitcast.12, bf16[768,2048]{0,1:T(8,128)(2,1)S(1)} %bitcast.223, bf16[2048,768]{1,0:T(8,128)(2,1)} %all-gather.3.cloned.1.call-done, f32[768,384]{1,0:T(8,128)} %convolution_multiply_fusion.2, f32[384]{0:T(512)S(1)} %copy-done.26), kind=kOutput, calls=%fused_computation.39 | convolution fusion | flops 2419556352 | bytes 10618368 | tf_op jit(solution)/shard_map/dot_general | solution.py:154
  344.5 2.1 copy.169
  346.6 47.0 %all_to_all.48 = bf16[8,768,256]{2,1,0:T(8,128)(2,1)S(1)} all-to-all(bf16[8,768,256]{2,1,0:T(8,128)(2,1)S(1)} %bitcast.215), channel_id=1, replica_groups=mesh['fs'=16,'tp'=8] {'tp'}, dimensions={0} | all-to-all | bytes 6291456 | tf_op jit(solution)/shard_map/all_to_all | solution.py:36
  (179 shorter events, 45.8 us)
Async XLA Ops:
  6.5 65.2 %all-gather.3.cloned.1.call-start = ((), (), s32[]{:S(2)}) async-start(), calls=%async_computation.8 | async-start | bytes 3342336 | tf_op jit(solution)/shard_map/all_gather | solution.py:43
  10.3 44.6 %copy-start.14 = (f32[128,256]{1,0:T(8,128)S(1)}, f32[128,256]{1,0:T(8,128)}, u32[]{:S(2)}) copy-start(f32[128,256]{1,0:T(8,128)} %param.33) | copy-start | bytes 393220
  20.8 34.2 %copy-start.15 = (f32[128,256]{1,0:T(8,128)S(1)}, f32[128,256]{1,0:T(8,128)}, u32[]{:S(2)}) copy-start(f32[128,256]{1,0:T(8,128)} %param.34) | copy-start | bytes 393220
  20.8 34.2 %copy-start.16 = (f32[128,256]{1,0:T(8,128)S(1)}, f32[128,256]{1,0:T(8,128)}, u32[]{:S(2)}) copy-start(f32[128,256]{1,0:T(8,128)} %param.35) | copy-start | bytes 393220
  22.0 33.0 %copy-start.17 = (f32[128,256]{1,0:T(8,128)S(1)}, f32[128,256]{1,0:T(8,128)}, u32[]{:S(2)}) copy-start(f32[128,256]{1,0:T(8,128)} %param.36) | copy-start | bytes 393220
  22.1 5.6 %collective-permute-start = (bf16[768,256]{1,0:T(8,128)(2,1)S(1)}, bf16[768,256]{1,0:T(8,128)(2,1)S(1)}, u32[]{:S(2)}, u32[]{:S(2)}) collective-permute-start(bf16[768,256]{1,0:T(8,128)(2,1)S(1)} %fusion.54), channel_id=1, source_target_pairs={{0,1},{1,2},{2,3},{3,4},{4,5},{5,6},{6,7},{7,0},{8,9},{9,10},{10,1... | collective-permute-start | bytes 1179656 | tf_op jit(solution)/shard_map/ppermute | solution.py:125
  27.7 7.2 %collective-permute-start.1 = (bf16[768,256]{1,0:T(8,128)(2,1)S(1)}, bf16[768,256]{1,0:T(8,128)(2,1)S(1)}, u32[]{:S(2)}, u32[]{:S(2)}) collective-permute-start(bf16[768,256]{1,0:T(8,128)(2,1)S(1)} %collective-permute-done), channel_id=1, source_target_pairs={{0,1},{1,2},{2,3},{3,4},{4,5},{5,6},{6,7},{7,0},{8,9},{9,10},{10,1... | collective-permute-start | bytes 1179656 | tf_op jit(solution)/shard_map/ppermute | solution.py:125
  30.2 7.5 %collective-permute-start.4 = (bf16[768,256]{1,0:T(8,128)(2,1)S(1)}, bf16[768,256]{1,0:T(8,128)(2,1)S(1)}, u32[]{:S(2)}, u32[]{:S(2)}) collective-permute-start(bf16[768,256]{1,0:T(8,128)(2,1)S(1)} %fusion.54), channel_id=1, source_target_pairs={{1,0},{2,1},{3,2},{4,3},{5,4},{6,5},{7,6},{0,7},{9,8},{10,9},{11,1... | collective-permute-start | bytes 1179656 | tf_op jit(solution)/shard_map/ppermute | solution.py:129
  34.9 7.2 %collective-permute-start.2 = (bf16[768,256]{1,0:T(8,128)(2,1)S(1)}, bf16[768,256]{1,0:T(8,128)(2,1)S(1)}, u32[]{:S(2)}, u32[]{:S(2)}) collective-permute-start(bf16[768,256]{1,0:T(8,128)(2,1)S(1)} %collective-permute-done.1), channel_id=1, source_target_pairs={{0,1},{1,2},{2,3},{3,4},{4,5},{5,6},{6,7},{7,0},{8,9},{9,10},{10,1... | collective-permute-start | bytes 1179656 | tf_op jit(solution)/shard_map/ppermute | solution.py:125
  37.7 18.2 %collective-permute-start.5 = (bf16[768,256]{1,0:T(8,128)(2,1)S(1)}, bf16[768,256]{1,0:T(8,128)(2,1)S(1)}, u32[]{:S(2)}, u32[]{:S(2)}) collective-permute-start(bf16[768,256]{1,0:T(8,128)(2,1)S(1)} %collective-permute-done.4), channel_id=1, source_target_pairs={{1,0},{2,1},{3,2},{4,3},{5,4},{6,5},{7,6},{0,7},{9,8},{10,9},{11,1... | collective-permute-start | bytes 1179656 | tf_op jit(solution)/shard_map/ppermute | solution.py:129
  42.1 17.5 %collective-permute-start.3 = (bf16[768,256]{1,0:T(8,128)(2,1)S(1)}, bf16[768,256]{1,0:T(8,128)(2,1)S(1)}, u32[]{:S(2)}, u32[]{:S(2)}) collective-permute-start(bf16[768,256]{1,0:T(8,128)(2,1)S(1)} %collective-permute-done.2), channel_id=1, source_target_pairs={{0,1},{1,2},{2,3},{3,4},{4,5},{5,6},{6,7},{7,0},{8,9},{9,10},{10,1... | collective-permute-start | bytes 1179656 | tf_op jit(solution)/shard_map/ppermute | solution.py:125
  47.0 30.1 %all-to-all-start.1 = ((bf16[16,384,128]{1,2,0:T(8,128)(2,1)}), bf16[16,384,128]{1,2,0:T(8,128)(2,1)}, u32[]{:S(2)}, u32[]{:S(2)}) async-start(bf16[16,384,128]{1,2,0:T(8,128)(2,1)} %broadcast_in_dim.24), calls=%async_computation.1 | async-start | bytes 3145728 | tf_op jit(solution)/shard_map/all_to_all | solution.py:21
  54.9 8.0 %copy-start = (bf16[768,256]{1,0:T(8,128)(2,1)S(1)}, bf16[768,256]{1,0:T(8,128)(2,1)}, u32[]{:S(2)}) copy-start(bf16[768,256]{1,0:T(8,128)(2,1)} %param.24) | copy-start | bytes 1179652
  54.9 8.0 %copy-start.18 = (f32[256]{0:T(256)S(1)}, f32[256]{0:T(256)}, u32[]{:S(2)}) copy-start(f32[256]{0:T(256)} %param.25) | copy-start | bytes 3076
  54.9 147.3 %all-gather.5.cloned.1.call-start = ((), (), s32[]{:S(2)}) async-start(), calls=%async_computation.9 | async-start | bytes 4456448 | tf_op jit(solution)/shard_map/all_gather | solution.py:43
  55.9 9.5 %collective-permute-start.6 = (bf16[768,256]{1,0:T(8,128)(2,1)S(1)}, bf16[768,256]{1,0:T(8,128)(2,1)S(1)}, u32[]{:S(2)}, u32[]{:S(2)}) collective-permute-start(bf16[768,256]{1,0:T(8,128)(2,1)S(1)} %collective-permute-done.5), channel_id=1, source_target_pairs={{1,0},{2,1},{3,2},{4,3},{5,4},{6,5},{7,6},{0,7},{9,8},{10,9},{11,1... | collective-permute-start | bytes 1179656 | tf_op jit(solution)/shard_map/ppermute | solution.py:129
  68.8 2.9 copy-start.23
  71.7 5.4 %copy-start.4 = (bf16[768,8,256]{0,2,1:T(8,128)(2,1)S(1)}, bf16[768,8,256]{0,2,1:T(8,128)(2,1)}, u32[]{:S(2)}) copy-start(bf16[768,8,256]{0,2,1:T(8,128)(2,1)} %copy.131) | copy-start | bytes 9437188
  71.7 5.4 %copy-start.25 = (f32[384]{0:T(512)S(1)}, f32[384]{0:T(512)}, u32[]{:S(2)}) copy-start(f32[384]{0:T(512)} %param.30) | copy-start | bytes 4612
  88.5 10.9 %copy-start.21 = (f32[256]{0:T(256)S(1)}, f32[256]{0:T(256)}, u32[]{:S(2)}) copy-start(f32[256]{0:T(256)} %param.31) | copy-start | bytes 3076
  88.5 48.3 %all-to-all-start.2 = ((bf16[8,768,256]{2,1,0:T(8,128)(2,1)}), bf16[8,768,256]{2,1,0:T(8,128)(2,1)S(1)}, u32[]{:S(2)}, u32[]{:S(2)}) async-start(bf16[8,768,256]{2,1,0:T(8,128)(2,1)} %bitcast.172), calls=%async_computation.2 | async-start | bytes 6291456 | tf_op jit(solution)/shard_map/all_to_all | solution.py:36
  99.4 46.2 %copy-start.19 = (f32[256]{0:T(256)S(1)}, f32[256]{0:T(256)}, u32[]{:S(2)}) copy-start(f32[256]{0:T(256)} %param.32) | copy-start | bytes 3076
  137.5 52.3 %copy-start.1 = (bf16[768,256]{1,0:T(8,128)(2,1)}, bf16[768,256]{1,0:T(8,128)(2,1)S(1)}, u32[]{:S(2)}) copy-start(bf16[768,256]{1,0:T(8,128)(2,1)S(1)} %get-tuple-element.218) | copy-start | bytes 1179652
  145.8 5.6 %collective-permute-start.7 = (bf16[768,256]{1,0:T(8,128)(2,1)S(1)}, bf16[768,256]{1,0:T(8,128)(2,1)S(1)}, u32[]{:S(2)}, u32[]{:S(2)}) collective-permute-start(bf16[768,256]{1,0:T(8,128)(2,1)S(1)} %fusion.58), channel_id=1, source_target_pairs={{0,1},{1,2},{2,3},{3,4},{4,5},{5,6},{6,7},{7,0},{8,9},{9,10},{10,1... | collective-permute-start | bytes 1179656 | tf_op jit(solution)/shard_map/ppermute | solution.py:125
  151.4 7.2 %collective-permute-start.8 = (bf16[768,256]{1,0:T(8,128)(2,1)S(1)}, bf16[768,256]{1,0:T(8,128)(2,1)S(1)}, u32[]{:S(2)}, u32[]{:S(2)}) collective-permute-start(bf16[768,256]{1,0:T(8,128)(2,1)S(1)} %collective-permute-done.7), channel_id=1, source_target_pairs={{0,1},{1,2},{2,3},{3,4},{4,5},{5,6},{6,7},{7,0},{8,9},{9,10},{10,1... | collective-permute-start | bytes 1179656 | tf_op jit(solution)/shard_map/ppermute | solution.py:125
  153.9 13.8 %collective-permute-start.11 = (bf16[768,256]{1,0:T(8,128)(2,1)S(1)}, bf16[768,256]{1,0:T(8,128)(2,1)S(1)}, u32[]{:S(2)}, u32[]{:S(2)}) collective-permute-start(bf16[768,256]{1,0:T(8,128)(2,1)S(1)} %fusion.58), channel_id=1, source_target_pairs={{1,0},{2,1},{3,2},{4,3},{5,4},{6,5},{7,6},{0,7},{9,8},{10,9},{11,1... | collective-permute-start | bytes 1179656 | tf_op jit(solution)/shard_map/ppermute | solution.py:129
  158.6 11.4 %collective-permute-start.9 = (bf16[768,256]{1,0:T(8,128)(2,1)S(1)}, bf16[768,256]{1,0:T(8,128)(2,1)S(1)}, u32[]{:S(2)}, u32[]{:S(2)}) collective-permute-start(bf16[768,256]{1,0:T(8,128)(2,1)S(1)} %collective-permute-done.8), channel_id=1, source_target_pairs={{0,1},{1,2},{2,3},{3,4},{4,5},{5,6},{6,7},{7,0},{8,9},{9,10},{10,1... | collective-permute-start | bytes 1179656 | tf_op jit(solution)/shard_map/ppermute | solution.py:125
  163.2 73.4 %all-to-all-start.4 = ((bf16[16,256,128]{1,2,0:T(8,128)(2,1)}), bf16[16,256,128]{1,2,0:T(8,128)(2,1)}, u32[]{:S(2)}, u32[]{:S(2)}) async-start(bf16[16,256,128]{1,2,0:T(8,128)(2,1)} %broadcast_in_dim.29), calls=%async_computation.4 | async-start | bytes 2097152 | tf_op jit(solution)/shard_map/all_to_all | solution.py:21
  167.7 15.8 %collective-permute-start.12 = (bf16[768,256]{1,0:T(8,128)(2,1)S(1)}, bf16[768,256]{1,0:T(8,128)(2,1)S(1)}, u32[]{:S(2)}, u32[]{:S(2)}) collective-permute-start(bf16[768,256]{1,0:T(8,128)(2,1)S(1)} %collective-permute-done.11), channel_id=1, source_target_pairs={{1,0},{2,1},{3,2},{4,3},{5,4},{6,5},{7,6},{0,7},{9,8},{10,9},{11,1... | collective-permute-start | bytes 1179656 | tf_op jit(solution)/shard_map/ppermute | solution.py:129
  170.0 16.5 %collective-permute-start.10 = (bf16[768,256]{1,0:T(8,128)(2,1)S(1)}, bf16[768,256]{1,0:T(8,128)(2,1)S(1)}, u32[]{:S(2)}, u32[]{:S(2)}) collective-permute-start(bf16[768,256]{1,0:T(8,128)(2,1)S(1)} %collective-permute-done.9), channel_id=1, source_target_pairs={{0,1},{1,2},{2,3},{3,4},{4,5},{5,6},{6,7},{7,0},{8,9},{9,10},{10,1... | collective-permute-start | bytes 1179656 | tf_op jit(solution)/shard_map/ppermute | solution.py:125
  183.5 8.7 %collective-permute-start.13 = (bf16[768,256]{1,0:T(8,128)(2,1)S(1)}, bf16[768,256]{1,0:T(8,128)(2,1)S(1)}, u32[]{:S(2)}, u32[]{:S(2)}) collective-permute-start(bf16[768,256]{1,0:T(8,128)(2,1)S(1)} %collective-permute-done.12), channel_id=1, source_target_pairs={{1,0},{2,1},{3,2},{4,3},{5,4},{6,5},{7,6},{0,7},{9,8},{10,9},{11,1... | collective-permute-start | bytes 1179656 | tf_op jit(solution)/shard_map/ppermute | solution.py:129
  197.4 4.8 %copy-start.27 = (f32[256]{0:T(256)S(1)}, f32[256]{0:T(256)}, u32[]{:S(2)}) copy-start(f32[256]{0:T(256)} %param.38) | copy-start | bytes 3076
  207.0 2.2 copy-start.3
  207.1 2.2 copy-start.28
  212.4 1.9 copy-start.13
  212.4 4.3 %copy-start.29 = (f32[256]{0:T(256)S(1)}, f32[256]{0:T(256)}, u32[]{:S(2)}) copy-start(f32[256]{0:T(256)} %param.39) | copy-start | bytes 3076
  216.7 3.4 copy-start.6
  216.7 3.4 copy-start.7
  216.7 3.5 copy-start.8
  216.7 3.5 copy-start.9
  216.7 3.5 copy-start.10
  216.7 3.5 copy-start.11
  216.8 3.5 copy-start.12
  222.0 11.2 %copy-start.30 = (f32[256]{0:T(256)S(1)}, f32[256]{0:T(256)}, u32[]{:S(2)}) copy-start(f32[256]{0:T(256)} %param.40) | copy-start | bytes 3076
  222.0 11.2 %copy-start.31 = (f32[256]{0:T(256)S(1)}, f32[256]{0:T(256)}, u32[]{:S(2)}) copy-start(f32[256]{0:T(256)} %param.41) | copy-start | bytes 3076
  283.1 1.0 copy-start.2
  283.1 1.0 copy-start.22
  283.1 9.4 %copy-start.20 = (f32[256]{0:T(256)S(1)}, f32[256]{0:T(256)}, u32[]{:S(2)}) copy-start(f32[256]{0:T(256)} %param.45) | copy-start | bytes 3076
  292.7 5.6 %collective-permute-start.14 = (bf16[768,256]{1,0:T(8,128)(2,1)S(1)}, bf16[768,256]{1,0:T(8,128)(2,1)S(1)}, u32[]{:S(2)}, u32[]{:S(2)}) collective-permute-start(bf16[768,256]{1,0:T(8,128)(2,1)S(1)} %fusion.62), channel_id=1, source_target_pairs={{0,1},{1,2},{2,3},{3,4},{4,5},{5,6},{6,7},{7,0},{8,9},{9,10},{10,1... | collective-permute-start | bytes 1179656 | tf_op jit(solution)/shard_map/ppermute | solution.py:125
  298.3 7.2 %collective-permute-start.15 = (bf16[768,256]{1,0:T(8,128)(2,1)S(1)}, bf16[768,256]{1,0:T(8,128)(2,1)S(1)}, u32[]{:S(2)}, u32[]{:S(2)}) collective-permute-start(bf16[768,256]{1,0:T(8,128)(2,1)S(1)} %collective-permute-done.14), channel_id=1, source_target_pairs={{0,1},{1,2},{2,3},{3,4},{4,5},{5,6},{6,7},{7,0},{8,9},{9,10},{10,1... | collective-permute-start | bytes 1179656 | tf_op jit(solution)/shard_map/ppermute | solution.py:125
  300.8 7.5 %collective-permute-start.18 = (bf16[768,256]{1,0:T(8,128)(2,1)S(1)}, bf16[768,256]{1,0:T(8,128)(2,1)S(1)}, u32[]{:S(2)}, u32[]{:S(2)}) collective-permute-start(bf16[768,256]{1,0:T(8,128)(2,1)S(1)} %fusion.62), channel_id=1, source_target_pairs={{1,0},{2,1},{3,2},{4,3},{5,4},{6,5},{7,6},{0,7},{9,8},{10,9},{11,1... | collective-permute-start | bytes 1179656 | tf_op jit(solution)/shard_map/ppermute | solution.py:129
  305.5 7.2 %collective-permute-start.16 = (bf16[768,256]{1,0:T(8,128)(2,1)S(1)}, bf16[768,256]{1,0:T(8,128)(2,1)S(1)}, u32[]{:S(2)}, u32[]{:S(2)}) collective-permute-start(bf16[768,256]{1,0:T(8,128)(2,1)S(1)} %collective-permute-done.15), channel_id=1, source_target_pairs={{0,1},{1,2},{2,3},{3,4},{4,5},{5,6},{6,7},{7,0},{8,9},{9,10},{10,1... | collective-permute-start | bytes 1179656 | tf_op jit(solution)/shard_map/ppermute | solution.py:125
  308.3 7.5 %collective-permute-start.19 = (bf16[768,256]{1,0:T(8,128)(2,1)S(1)}, bf16[768,256]{1,0:T(8,128)(2,1)S(1)}, u32[]{:S(2)}, u32[]{:S(2)}) collective-permute-start(bf16[768,256]{1,0:T(8,128)(2,1)S(1)} %collective-permute-done.18), channel_id=1, source_target_pairs={{1,0},{2,1},{3,2},{4,3},{5,4},{6,5},{7,6},{0,7},{9,8},{10,9},{11,1... | collective-permute-start | bytes 1179656 | tf_op jit(solution)/shard_map/ppermute | solution.py:129
  312.7 7.2 %collective-permute-start.17 = (bf16[768,256]{1,0:T(8,128)(2,1)S(1)}, bf16[768,256]{1,0:T(8,128)(2,1)S(1)}, u32[]{:S(2)}, u32[]{:S(2)}) collective-permute-start(bf16[768,256]{1,0:T(8,128)(2,1)S(1)} %collective-permute-done.16), channel_id=1, source_target_pairs={{0,1},{1,2},{2,3},{3,4},{4,5},{5,6},{6,7},{7,0},{8,9},{9,10},{10,1... | collective-permute-start | bytes 1179656 | tf_op jit(solution)/shard_map/ppermute | solution.py:125
  315.8 9.7 %collective-permute-start.20 = (bf16[768,256]{1,0:T(8,128)(2,1)S(1)}, bf16[768,256]{1,0:T(8,128)(2,1)S(1)}, u32[]{:S(2)}, u32[]{:S(2)}) collective-permute-start(bf16[768,256]{1,0:T(8,128)(2,1)S(1)} %collective-permute-done.19), channel_id=1, source_target_pairs={{1,0},{2,1},{3,2},{4,3},{5,4},{6,5},{7,6},{0,7},{9,8},{10,9},{11,1... | collective-permute-start | bytes 1179656 | tf_op jit(solution)/shard_map/ppermute | solution.py:129
  329.0 2.8 copy-start.24
  331.8 5.4 %copy-start.5 = (bf16[768,8,256]{0,2,1:T(8,128)(2,1)S(1)}, bf16[768,8,256]{0,2,1:T(8,128)(2,1)}, u32[]{:S(2)}) copy-start(bf16[768,8,256]{0,2,1:T(8,128)(2,1)} %copy.150) | copy-start | bytes 9437188
  331.8 5.4 %copy-start.26 = (f32[384]{0:T(512)S(1)}, f32[384]{0:T(512)}, u32[]{:S(2)}) copy-start(f32[384]{0:T(512)} %param.30) | copy-start | bytes 4612
Sparse Core Ops, SparseCore 0:
  9.5 51.8 all-gather.2
  63.5 64.2 all-gather.4
